TPU v7x, 32 devices: a whole 2x2x4 slice. The times are simulated.
32 devices in a mesh: grp: 2 (over y), ep: 8 (over z, core), tp: 2 (over x).
Axes of the slice: x: 2, y: 2, z: 4, core: 2. Of those that a mesh axis runs over, the one named last changes fastest.
Arguments:
- resid_in: bfloat16 [176, 2048], P(('grp', 'ep')), parts along dimension 0, may hold values from -6 to 6
- norm_attn: float32 [2048], replicated, may hold values from 0.1 to 1.9
- norm_moe: float32 [2048], replicated, may hold values from 0.1 to 1.9
- w_query: bfloat16 [2048, 1024], P('ep', 'tp'), may hold values from -0.125 to 0.125
- w_key: bfloat16 [2048, 256], P('ep', 'tp'), may hold values from -0.125 to 0.125
- w_value: bfloat16 [2048, 256], P('ep', 'tp'), may hold values from -0.125 to 0.125
- head_offset: float32 [16], P('tp'), may hold values from 1.5 to 9.5
- kv_cache: bfloat16 [176, 1024, 4, 128], P(('grp', 'ep'), None, 'tp'), parts along dimension 0, may hold values from -6 to 6
- lengths: int32 [176], P(('grp', 'ep')), parts along dimension 0, may hold values from 128 to 1024, as said below
- w_output: bfloat16 [1024, 2048], P('tp', 'ep'), may hold values from -0.375 to 0.375
- routes: int32 [176, 4], P(('grp', 'ep')), parts along dimension 0, may hold values from 0 to 7, all different within a row; in each aligned block of 11 rows (0 to 10, 11 to 21, ...) at most 7 rows name the same one
- route_weights: float32 [176, 4], P(('grp', 'ep')), parts along dimension 0, may hold values from 0.2 to 1
- gate_experts: bfloat16 [8, 2048, 512], P('ep', None, 'tp'), may hold values from -0.125 to 0.125
- up_experts: bfloat16 [8, 2048, 512], P('ep', None, 'tp'), may hold values from -0.125 to 0.125
- down_experts: bfloat16 [8, 512, 2048], P('ep', 'tp'), may hold values from -0.25 to 0.25
- gate_shared: bfloat16 [2048, 512], P('ep', 'tp'), may hold values from -0.125 to 0.125
- up_shared: bfloat16 [2048, 512], P('ep', 'tp'), may hold values from -0.125 to 0.125
- down_shared: bfloat16 [512, 2048], P('tp', 'ep'), may hold values from -0.25 to 0.25
Outputs:
- layer_out: bfloat16 [176, 2048], P(('grp', 'ep'), 'tp'), parts along dimension 0
- new_rows: bfloat16 [176, 4, 128], P(('grp', 'ep'), 'tp'), parts along dimension 0
There are 2 independent parts, one for each index of `grp`. A program takes and returns all parts, laid end to end along the dimension named above; an argument that names none is the same for every part. Nothing has to cross between parts.
Inputs may be any that keep to these rules, and one draw needn't show every extreme that they name: `routes`: among the rows of one device no expert is named more than 7 times, and in every draw some expert is named exactly 7 times by one device's rows; a row names 4 different experts. Sequence b's new token follows cache positions 0 to lengths[b] - 1; the other positions are not read.
All inputs are finite; a program needn't handle non-finite values.
Results may differ from a plain program's by a relative error of at most 0.015.
Values may be sent and summed in bfloat16 or wider, within the bound.
A program may use at most 64 MiB of HBM per device.

v0:
```python
import jax
import jax.numpy as jnp
from jax import lax
from jax.sharding import PartitionSpec as P

HEAD = 64
TOPK = 4


EPS = 1e-06


def rms_scale(row_block, gain):
    rows_wide = row_block.astype(jnp.float32)
    inverse = lax.rsqrt(jnp.mean(rows_wide * rows_wide, axis=-1, keepdims=True) + EPS)
    return rows_wide * inverse * gain


def stick_read(query, kv_cache, lengths, offsets):
    seq_count = query.shape[0]
    kv_local = kv_cache.shape[2]
    head_local = offsets.shape[0]
    per_group = head_local // kv_local
    cache_len = kv_cache.shape[1]
    grouped = query.reshape(seq_count, kv_local, per_group, HEAD)
    key_rows = kv_cache[:, :, :, :HEAD]
    value_rows = kv_cache[:, :, :, HEAD:]
    scores = jnp.einsum("skgd,slkd->skgl", grouped, key_rows, preferred_element_type=jnp.float32)
    scores = scores * HEAD ** (-0.5) - offsets.reshape(1, kv_local, per_group, 1)
    positions = lax.broadcasted_iota(jnp.int32, (seq_count, cache_len), 1)
    alive_mask = (positions < lengths[:, None])[:, None, None, :]
    remain = jnp.where(alive_mask, jax.nn.log_sigmoid(-scores), 0.0)
    suffix = lax.cumsum(remain, axis=3, reverse=True) - remain
    stick = jnp.where(alive_mask, jnp.exp(jax.nn.log_sigmoid(scores) + suffix), 0.0).astype(
        jnp.bfloat16
    )
    mixed_out = jnp.einsum("skgl,slkd->skgd", stick, value_rows, preferred_element_type=jnp.float32)
    return mixed_out.reshape(seq_count, head_local * HEAD).astype(jnp.bfloat16)


def on_device(
    resid_in,
    norm_attn,
    norm_moe,
    w_query,
    w_key,
    w_value,
    head_offset,
    kv_cache,
    lengths,
    w_output,
    routes,
    route_weights,
    gate_experts,
    up_experts,
    down_experts,
    gate_shared,
    up_shared,
    down_shared,
):
    tok_count = resid_in.shape[0]
    n_ep = lax.axis_size("ep")
    normed = rms_scale(resid_in, norm_attn).astype(jnp.bfloat16)
    k_cols = w_key.shape[1]
    pieces = (
        lax.all_gather(w_query, "ep", axis=0, tiled=True),
        lax.all_gather(w_key, "ep", axis=0, tiled=True),
        lax.all_gather(w_value, "ep", axis=0, tiled=True),
    )
    sliced = normed
    query_f, key_f, value_f = tuple(
        (
            jnp.dot(sliced, weight_piece, preferred_element_type=jnp.float32)
            for weight_piece in pieces
        )
    )
    query = query_f.astype(jnp.bfloat16)
    kv_local = k_cols // HEAD
    key_new = key_f.astype(jnp.bfloat16).reshape(tok_count, kv_local, HEAD)
    value_new = value_f.astype(jnp.bfloat16).reshape(tok_count, kv_local, HEAD)
    new_rows = jnp.concatenate([key_new, value_new], axis=2)
    attended = stick_read(query, kv_cache, lengths, head_offset)
    attn_part = jnp.dot(
        attended,
        lax.all_gather(w_output, "ep", axis=1, tiled=True),
        preferred_element_type=jnp.float32,
    ).astype(jnp.bfloat16)
    attn_sum = lax.psum(attn_part, "tp").astype(jnp.float32)
    resid_mid = (resid_in.astype(jnp.float32) + attn_sum).astype(jnp.bfloat16)
    normed_moe = rms_scale(resid_mid, norm_moe).astype(jnp.bfloat16)
    pieces = (
        lax.all_gather(gate_shared, "ep", axis=0, tiled=True),
        lax.all_gather(up_shared, "ep", axis=0, tiled=True),
    )
    sliced = normed_moe
    gate_s = jnp.dot(sliced, pieces[0], preferred_element_type=jnp.float32)
    up_s = jnp.dot(sliced, pieces[1], preferred_element_type=jnp.float32)
    hidden_shared = (jax.nn.silu(gate_s) * up_s).astype(jnp.bfloat16)
    shared_part = jnp.dot(
        hidden_shared,
        lax.all_gather(down_shared, "ep", axis=1, tiled=True),
        preferred_element_type=jnp.float32,
    ).astype(jnp.bfloat16)
    shared_out = lax.psum_scatter(shared_part, "tp", scatter_dimension=1, tiled=True).astype(
        jnp.float32
    )
    local_experts = gate_experts.shape[0]
    experts_all = local_experts * n_ep
    capacity = min(tok_count, tok_count * TOPK // experts_all + 2)
    flat_routes = routes.reshape(-1)
    expert_ids = lax.broadcasted_iota(jnp.int32, (1, experts_all), 1)
    onehot = (flat_routes[:, None] == expert_ids).astype(jnp.int32)
    slots = jnp.sum((jnp.cumsum(onehot, axis=0) - onehot) * onehot, axis=1)
    expert_grid = lax.broadcasted_iota(jnp.int32, (experts_all, capacity, 1), 0)
    slot_grid = lax.broadcasted_iota(jnp.int32, (experts_all, capacity, 1), 1)
    match = (
        (flat_routes[None, None, :] == expert_grid) & (slots[None, None, :] == slot_grid)
    ).astype(jnp.bfloat16)
    source_rows = jnp.repeat(normed_moe, TOPK, axis=0)
    outgoing = jnp.einsum(
        "ecr,rd->ecd", match, source_rows, preferred_element_type=jnp.float32
    ).astype(jnp.bfloat16)
    arrived = lax.all_to_all(outgoing, "ep", split_axis=0, concat_axis=0, tiled=True)
    slot_count = arrived.shape[1]
    grouped_in = arrived.reshape(n_ep, local_experts, slot_count, arrived.shape[2])
    gate_h = jnp.einsum(
        "secd,edf->secf", grouped_in, gate_experts, preferred_element_type=jnp.float32
    )
    up_h = jnp.einsum("secd,edf->secf", grouped_in, up_experts, preferred_element_type=jnp.float32)
    hidden_e = (jax.nn.silu(gate_h) * up_h).astype(jnp.bfloat16)
    down_h = jnp.einsum(
        "secf,efd->secd", hidden_e, down_experts, preferred_element_type=jnp.float32
    ).astype(jnp.bfloat16)
    summed = (
        lax.psum_scatter(down_h, "tp", scatter_dimension=3, tiled=True)
        .astype(jnp.float32)
        .astype(jnp.bfloat16)
    )
    summed = summed.reshape(n_ep * local_experts, slot_count, summed.shape[3])
    returned = lax.all_to_all(summed, "ep", split_axis=0, concat_axis=0, tiled=True)
    gathered_back = jnp.einsum("ecr,ecd->rd", match, returned, preferred_element_type=jnp.float32)
    col_width = gathered_back.shape[1]
    weighted = gathered_back.reshape(tok_count, TOPK, col_width) * route_weights[:, :, None]
    routed = jnp.sum(weighted, axis=1)
    own_cols = lax.dynamic_slice_in_dim(resid_mid, lax.axis_index("tp") * col_width, col_width, 1)
    layer_out = (own_cols.astype(jnp.float32) + shared_out + routed).astype(jnp.bfloat16)
    return (layer_out, new_rows)


def solution(mesh):
    return jax.shard_map(
        on_device,
        mesh=mesh,
        in_specs=(
            P(("grp", "ep"), None),
            P(),
            P(),
            P("ep", "tp"),
            P("ep", "tp"),
            P("ep", "tp"),
            P("tp"),
            P(("grp", "ep"), None, "tp", None),
            P(("grp", "ep")),
            P("tp", "ep"),
            P(("grp", "ep"), None),
            P(("grp", "ep"), None),
            P("ep", None, "tp"),
            P("ep", None, "tp"),
            P("ep", "tp", None),
            P("ep", "tp"),
            P("ep", "tp"),
            P("tp", "ep"),
        ),
        out_specs=(P(("grp", "ep"), "tp"), P(("grp", "ep"), "tp", None)),
        check_vma=False,
    )
```

profile of v0, /device:TPU:0, one launch (start us, length us, event | category | flops | bytes accessed | tf_op | source)
XLA Modules:
  0.0 270.2 jit_solution(16846753004733863255)
XLA Ops:
  7.2 0.7 all-gather.6.cloned.1.call-update
  8.0 0.7 all-gather.8.cloned.1.call-update
  8.7 0.7 all-gather.10.cloned.1.call-update
  9.4 1.0 fusion.33
  10.5 12.9 %fusion.66 = (bf16[11,1024,2,64]{3,2,1,0:T(2,128)(2,1)}, bf16[11,1024,2,64]{3,2,1,0:T(2,128)(2,1)}) fusion(bf16[11,1024,2,128]{3,2,1,0:T(2,128)(2,1)} %param.25), kind=kLoop, calls=%fused_computation.81 | loop fusion | bytes 11534336 | tf_op jit(solution)/shard_map/slice | solution.py:26
  24.1 17.4 %all-gather.6.cloned.1.call-done = bf16[2048,512]{1,0:T(8,128)(2,1)} async-done(((bf16[256,512]{1,0:T(8,128)(2,1)}), bf16[2048,512]{1,0:T(8,128)(2,1)}) %all-gather.6.cloned.1.call-update) | async-done | bytes 2097168 | tf_op jit(solution)/shard_map/all_gather | solution.py:66
  41.5 2.0 convolution_convert_fusion.4
  43.6 4.3 %fusion.26 = (f32[11,2,4,1024]{3,2,1,0:T(4,128)S(1)}, f32[11,2,4,1024]{3,2,1,0:T(4,128)S(1)}) fusion(pred[11,1024]{1,0:T(8,128)(4,1)S(1)} %iota_compare_fusion, f32[2,4]{1,0:T(2,128)S(1)} %sub.16, bf16[11,2,4,64]{3,2,1,0:T(4,128)(2,1)S(1)} %reshape.94, bf16[11,1024,2,64]{3,2,1,0:T(2,128)(2,1)} %get-tuple-element.4), kind=kOutput, calls=%fused_computation.31 | convolution fusion | flops 12435456 | bytes 3627040 | tf_op jit(solution)/shard_map/skgd,slkd->skgl/dot_general | solution.py:28
  48.0 108.9 %reduce-window.6 = f32[11,2,4,8,128]{4,3,2,1,0:T(8,128)S(1)} reduce-window(f32[11,2,4,8,128]{4,3,2,1,0:T(8,128)S(1)} %reshape.95, f32[]{:T(128)} %constant.15.clone.1), window={size=1x1x1x1x128 pad=0_0x0_0x0_0x0_0x0_127}, to_apply=%region_1.2 | reduce-window | flops 11444224 | bytes 720900 | tf_op jit(solution)/shard_map/reduce-window
  157.0 0.5 copy.31
  158.0 4.4 %fusion.11 = bf16[11,2,4,64]{3,2,1,0:T(4,128)(2,1)S(1)} fusion(bf16[11,1024,2,64]{3,2,1,0:T(2,128)(2,1)} %get-tuple-element.5, f32[11,2,4,1024]{3,2,1,0:T(4,128)S(1)} %reduce_window_sum.26, f32[11,2,4,1024]{3,2,1,0:T(4,128)S(1)} %get-tuple-element.7, pred[11,1024]{1,0:T(8,128)(4,1)S(1)} %iota_compare_fusion), kind=kOutput, calls=%fused_computation.12 | convolution fusion | flops 13342208 | bytes 3627008 | tf_op jit(solution)/shard_map/skgl,slkd->skgd/dot_general | solution.py:37
  162.5 2.0 convolution_convert_fusion.3
  164.5 8.8 %psum.7 = bf16[11,2048]{1,0:T(8,128)(2,1)S(1)} all-reduce(bf16[11,2048]{1,0:T(8,128)(2,1)S(1)} %convolution_convert_fusion.3), channel_id=1, replica_groups=mesh['grp'=2,'ep'=8,'tp'=2] {'tp'}, use_global_device_ids=true, to_apply=%region_3.4 | all-reduce | flops 22528 | bytes 90112 | tf_op jit(solution)/shard_map/psum | solution.py:88
  174.0 12.6 %all_to_all.10 = bf16[8,7,2048]{2,1,0:T(8,128)(2,1)S(1)} all-to-all(bf16[8,7,2048]{2,1,0:T(8,128)(2,1)S(1)} %copy.35), channel_id=1, replica_groups=mesh['grp'=2,'ep'=8,'tp'=2] {'ep'}, dimensions={0} | all-to-all | bytes 458752 | tf_op jit(solution)/shard_map/all_to_all | solution.py:123
  186.6 0.3 fusion.16
  187.0 1.6 fusion.18
  188.5 1.0 fusion.4
  189.6 0.5 all-gather.12.cloned.1.call-update
  190.2 0.5 all-gather.14.cloned.1.call-update
  190.8 14.9 %all_gather.26 = bf16[2048,128]{1,0:T(8,128)(2,1)S(1)} all-gather(bf16[256,128]{1,0:T(8,128)(2,1)S(1)} %copy-done.4), channel_id=1, replica_groups=mesh['grp'=2,'ep'=8,'tp'=2] {'ep'}, dimensions={0}, use_global_device_ids=true | all-gather | bytes 589824 | tf_op jit(solution)/shard_map/all_gather | solution.py:67
  205.8 0.2 convolution_convert_fusion.6
  206.1 16.9 %all_gather.27 = bf16[2048,128]{1,0:T(8,128)(2,1)S(1)} all-gather(bf16[256,128]{1,0:T(8,128)(2,1)S(1)} %copy-done.5), channel_id=1, replica_groups=mesh['grp'=2,'ep'=8,'tp'=2] {'ep'}, dimensions={0}, use_global_device_ids=true | all-gather | bytes 589824 | tf_op jit(solution)/shard_map/all_gather | solution.py:68
  223.0 0.2 convolution_convert_fusion.5
  223.3 0.7 pad_maximum_fusion
  224.0 1.5 fusion.67
  225.5 1.6 copy.38
  227.1 3.4 %all-to-all-start.1 = ((bf16[8,7,1024]{2,1,0:T(8,128)(2,1)}), bf16[8,7,1024]{2,1,0:T(8,128)(2,1)S(1)}, u32[]{:S(2)}, u32[]{:S(2)}) async-start(bf16[8,7,1024]{2,1,0:T(8,128)(2,1)} %copy.38), calls=%async_computation.3 | async-start | bytes 262144 | tf_op jit(solution)/shard_map/all_to_all | solution.py:140
  230.5 19.6 %all-gather.14.cloned.1.call-done = bf16[256,2048]{1,0:T(8,128)(2,1)} async-done(((bf16[256,256]{1,0:T(8,128)(2,1)}), bf16[256,2048]{1,0:T(8,128)(2,1)}) %all-gather.14.cloned.1.call-update) | async-done | bytes 1048592 | tf_op jit(solution)/shard_map/all_gather | solution.py:101
  250.1 2.9 %convolution_convert_fusion.2 = bf16[11,2048]{1,0:T(8,128)(2,1)} fusion(bf16[256,2048]{1,0:T(8,128)(2,1)} %all-gather.14.cloned.1.call-done, bf16[11,2048]{1,0:T(8,128)(2,1)S(1)} %fusion.32, bf16[2048,256]{1,0:T(8,128)(2,1)} %all-gather.12.cloned.1.call-done, f32[11,256]{1,0:T(8,128)S(1)} %fusion.67), kind=kOutput, calls=%fused_computation.7 | convolution fusion | flops 23108096 | bytes 2198528 | tf_op jit(solution)/shard_map/dot_general | solution.py:99
  253.1 0.2 convolution_bitcast_fusion
  253.5 8.5 %reduce-scatter.3.cloned.1.call-done = bf16[11,1024]{1,0:T(8,128)(2,1)} async-done(((bf16[11,2048]{1,0:T(8,128)(2,1)}), bf16[11,1024]{1,0:T(8,128)(2,1)}) %reduce-scatter.3.cloned.1.call-update) | async-done | bytes 22544 | tf_op jit(solution)/shard_map/reduce_scatter | solution.py:104
  262.0 1.4 add_convert_fusion
  (64 shorter events, 3.1 us)
Async XLA Ops:
  7.2 181.4 %copy-start = (bf16[1,256,2048]{2,1,0:T(8,128)(2,1)S(1)}, bf16[1,256,2048]{2,1,0:T(8,128)(2,1)}, u32[]{:S(2)}) copy-start(bf16[1,256,2048]{2,1,0:T(8,128)(2,1)} %param.32) | copy-start | bytes 3145732
  7.2 34.3 %all-gather.6.cloned.1.call-start = ((), (), s32[]{:S(2)}) async-start(), calls=%async_computation.4 | async-start | bytes 2359296 | tf_op jit(solution)/shard_map/all_gather | solution.py:66
  7.9 154.6 %all-gather.8.cloned.1.call-start = ((), (), s32[]{:S(2)}) async-start(), calls=%async_computation.5 | async-start | bytes 2359296 | tf_op jit(solution)/shard_map/all_gather | solution.py:85
  8.7 215.3 %all-gather.10.cloned.1.call-start = ((), (), s32[]{:S(2)}) async-start(), calls=%async_computation.6 | async-start | bytes 1179648 | tf_op jit(solution)/shard_map/all_gather | solution.py:92
  9.4 216.1 %reduce-scatter.5.cloned.1.call-start = ((), (), s32[]{:S(2)}) async-start(), calls=%async_computation.10 | async-start | bytes 344064 | tf_op jit(solution)/shard_map/reduce_scatter | solution.py:135
  10.4 13.0 %copy-start.9 = (s32[11]{0:T(128)S(1)}, s32[11]{0:T(128)}, u32[]{:S(2)}) copy-start(s32[11]{0:T(128)} %param.26) | copy-start | bytes 136
  10.4 13.1 %copy-start.10 = (f32[8]{0:T(128)S(1)}, f32[8]{0:T(128)}, u32[]{:S(2)}) copy-start(f32[8]{0:T(128)} %param.24) | copy-start | bytes 100
  10.4 13.2 %copy-start.7 = (s32[11,4]{0,1:T(4,128)S(1)}, s32[11,4]{0,1:T(4,128)}, u32[]{:S(2)}) copy-start(s32[11,4]{0,1:T(4,128)} %param.28) | copy-start | bytes 532
  10.5 31.0 %copy-start.1 = (bf16[11,2048]{1,0:T(8,128)(2,1)S(1)}, bf16[11,2048]{1,0:T(8,128)(2,1)}, u32[]{:S(2)}) copy-start(bf16[11,2048]{1,0:T(8,128)(2,1)} %param.18) | copy-start | bytes 135172
  10.5 31.0 %copy-start.3 = (f32[2048]{0:T(1024)S(1)}, f32[2048]{0:T(1024)}, u32[]{:S(2)}) copy-start(f32[2048]{0:T(1024)} %param.19) | copy-start | bytes 24580
  158.0 15.5 %copy-start.6 = (f32[2048]{0:T(1024)S(1)}, f32[2048]{0:T(1024)}, u32[]{:S(2)}) copy-start(f32[2048]{0:T(1024)} %param.20) | copy-start | bytes 24580
  158.0 28.6 %copy-start.2 = (bf16[1,2048,256]{2,1,0:T(8,128)(2,1)S(1)}, bf16[1,2048,256]{2,1,0:T(8,128)(2,1)}, u32[]{:S(2)}) copy-start(bf16[1,2048,256]{2,1,0:T(8,128)(2,1)} %param.31) | copy-start | bytes 3145732
  162.4 28.4 %copy-start.8 = (f32[11,4]{0,1:T(4,128)S(1)}, f32[11,4]{0,1:T(4,128)}, u32[]{:S(2)}) copy-start(f32[11,4]{0,1:T(4,128)} %param.29) | copy-start | bytes 532
  162.4 28.5 %copy-start.4 = (bf16[256,128]{1,0:T(8,128)(2,1)S(1)}, bf16[256,128]{1,0:T(8,128)(2,1)}, u32[]{:S(2)}) copy-start(bf16[256,128]{1,0:T(8,128)(2,1)} %param.22) | copy-start | bytes 196612
  162.4 43.7 %copy-start.5 = (bf16[256,128]{1,0:T(8,128)(2,1)S(1)}, bf16[256,128]{1,0:T(8,128)(2,1)}, u32[]{:S(2)}) copy-start(bf16[256,128]{1,0:T(8,128)(2,1)} %param.23) | copy-start | bytes 196612
  189.6 41.0 %all-gather.12.cloned.1.call-start = ((), (), s32[]{:S(2)}) async-start(), calls=%async_computation.7 | async-start | bytes 1179648 | tf_op jit(solution)/shard_map/all_gather | solution.py:93
  190.2 60.0 %all-gather.14.cloned.1.call-start = ((), (), s32[]{:S(2)}) async-start(), calls=%async_computation.8 | async-start | bytes 1179648 | tf_op jit(solution)/shard_map/all_gather | solution.py:101
  227.1 26.0 %all-to-all-start.1 = ((bf16[8,7,1024]{2,1,0:T(8,128)(2,1)}), bf16[8,7,1024]{2,1,0:T(8,128)(2,1)S(1)}, u32[]{:S(2)}, u32[]{:S(2)}) async-start(bf16[8,7,1024]{2,1,0:T(8,128)(2,1)} %copy.38), calls=%async_computation.3 | async-start | bytes 262144 | tf_op jit(solution)/shard_map/all_to_all | solution.py:140
  230.5 31.5 %reduce-scatter.3.cloned.1.call-start = ((), (), s32[]{:S(2)}) async-start(), calls=%async_computation.9 | async-start | bytes 98304 | tf_op jit(solution)/shard_map/reduce_scatter | solution.py:104
Sparse Core Ops, SparseCore 0:
  9.6 31.8 all-gather.5
  43.1 30.0 all-gather.7
  74.8 21.2 all-gather.9
  189.7 9.3 reduce-scatter.4
  200.5 24.5 all-gather.11
  226.6 23.5 all-gather.13
  253.2 8.7 reduce-scatter.2
where the time goes:
time: 271 us; the launch traced here: 270 us
  other arithmetic  113 us (42%)
  blocking collectives  53.2 us (20%)
  waiting for transfers between devices  48.6 us (18%)
  matrix products  20.8 us (8%)
  local copies, waits for them, and re-layouts  16.5 us (6%)
  between operations  14.4 us (5%)
  starting transfers between devices  3.64 us (1%)
    another operation x2, other arithmetic  109 us
    all_gather x1, waiting for transfers between devices, on_device(): lax.all_gather(down_shared, 'ep', axis=1, tiled=True)  19.6 us
    all_gather x1, waiting for transfers between devices, on_device(): lax.all_gather(w_query, 'ep', axis=0, tiled=True)  17.4 us
    all_gather x1, blocking collectives, on_device(): lax.all_gather(w_value, 'ep', axis=0, tiled=True)  16.9 us
    all_gather x1, blocking collectives, on_device(): lax.all_gather(w_key, 'ep', axis=0, tiled=True)  14.9 us
    slice x1, local copies, waits for them, and re-layouts, stick_read(): key_rows = kv_cache[:, :, :, :HEAD]  12.9 us
    all_to_all x1, blocking collectives, on_device(): lax.all_to_all(outgoing, 'ep', split_axis=0, concat_axis=0, tiled=True)  12.6 us
    psum x1, blocking collectives, on_device(): attn_sum = lax.psum(attn_part, 'tp').astype(jnp.float32)  8.79 us
  transfers between devices with their start and end apart: 8, of which 3 were waited for; matrix products, arithmetic and copies ran while one was open for 55% of the time, Pallas kernels for 0%

commit v1 on v0

--- a/solution.py
+++ b/solution.py
@@ -1,6 +1,10 @@
+import functools
+
 import jax
 import jax.numpy as jnp
 from jax import lax
+from jax.experimental import pallas as pl
+from jax.experimental.pallas import tpu as pltpu
 from jax.sharding import PartitionSpec as P
 
 HEAD = 64
@@ -147,9 +151,370 @@
     return (layer_out, new_rows)
 
 
+MESH = pl.DeviceIdType.MESH
+ROWS = 16
+SLOTS = 8
+BF = jnp.bfloat16
+F32 = jnp.float32
+
+
+def fdot(a, b):
+    return jnp.dot(a, b, preferred_element_type=F32)
+
+
+def iota(shape, dim):
+    return lax.broadcasted_iota(jnp.int32, shape, dim)
+
+
+def layer_kernel(
+    n, n_tp, tok, resid, g_attn, g_moe, offs, lens, routes, rweights,
+    wq_h, wk_h, wv_h, kv_h, wo_h, ge_h, ue_h, de_h, gs_h, us_h, ds_h,
+    out, new_rows,
+    wqkv, kv, wo, ge, ue, de, gus, dsh,
+    x32, xs, xr, p2s, p2r, sc, st, oh, ags, agr, p5s, p5r, rm, dsp, dsr, nss, nsr,
+    s1s, s1r, hs, hr, fs, fr, f2s, f2r, rts, rws,
+    lsem, s_p1, r_p1, s_p2, r_p2, s_ag, r_ag, s_p5, r_p5, s_d, r_d, s_n, r_n,
+    s_s1, r_s1, s_s2, r_s2, s_f, r_f, s_f2, r_f2,
+):
+    me = lax.axis_index("ep")
+    tp = lax.axis_index("tp")
+    d_model = x32.shape[1]
+    width = d_model // n
+    qcols = wq_h.shape[1]
+    kcols = wk_h.shape[1]
+    heads = offs.shape[1]
+    kv_local = kcols // HEAD
+    per_group = heads // kv_local
+    span = kv_h.shape[1]
+    allrows = n * ROWS
+
+    loads = []
+
+    def load(src, dst):
+        copy = pltpu.make_async_copy(src, dst, lsem.at[len(loads)])
+        copy.start()
+        loads.append(copy)
+        return copy
+
+    l_qkv = [
+        load(wq_h, wqkv.at[:, pl.ds(0, qcols)]),
+        load(wk_h, wqkv.at[:, pl.ds(qcols, kcols)]),
+        load(wv_h, wqkv.at[:, pl.ds(qcols + kcols, kcols)]),
+    ]
+    l_kv = [load(kv_h.at[s], kv.at[s]) for s in range(tok)]
+    l_wo = load(wo_h, wo)
+    fs_cols = gs_h.shape[1]
+    l_gus = [load(gs_h, gus.at[:, pl.ds(0, fs_cols)]), load(us_h, gus.at[:, pl.ds(fs_cols, fs_cols)])]
+    l_exp = [load(ge_h.at[0], ge), load(ue_h.at[0], ue), load(de_h.at[0], de)]
+    l_ds = load(ds_h, dsh)
+
+    barrier = pltpu.get_barrier_semaphore()
+    for t in range(n_tp):
+        for k in range(n):
+            if t or k:
+                pl.semaphore_signal(
+                    barrier,
+                    inc=1,
+                    device_id={"ep": lax.rem(me + k, n), "tp": lax.rem(tp + t, n_tp)},
+                    device_id_type=MESH,
+                )
+
+    x32[...] = jnp.zeros_like(x32)
+    x32[0:tok, :] = resid[...].astype(F32)
+    for j in range(n):
+        xs[j] = x32[:, j * width : (j + 1) * width].astype(BF)
+    xr[me] = xs[me]
+    rts[...] = jnp.full(rts.shape, -1, jnp.int32)
+    rts[:, 0:tok] = routes[...]
+    rws[...] = jnp.zeros_like(rws)
+    rws[:, 0:tok] = rweights[...]
+
+    pl.semaphore_wait(barrier, n * n_tp - 1)
+
+    sent = []
+
+    def exchange(src, dst, ssem, rsem):
+        arrivals = []
+        for k in range(1, n):
+            peer = lax.rem(me + k, n)
+            copy = pltpu.make_async_remote_copy(
+                src_ref=src(peer), dst_ref=dst(me), send_sem=ssem.at[k], recv_sem=rsem.at[k],
+                device_id={"ep": peer}, device_id_type=MESH,
+            )
+            copy.start()
+            sent.append(copy)
+            origin = lax.rem(me + n - k, n)
+            arrivals.append(
+                pltpu.make_async_remote_copy(
+                    src_ref=src(peer), dst_ref=dst(origin), send_sem=ssem.at[k], recv_sem=rsem.at[k],
+                    device_id={"ep": peer}, device_id_type=MESH,
+                )
+            )
+        return arrivals
+
+    def exchange_tp(src, dst, ssem, rsem):
+        arrivals = []
+        for k in range(n):
+            for t in range(n_tp):
+                if not (k or t):
+                    continue
+                peer = lax.rem(me + k, n)
+                peer_tp = lax.rem(tp + t, n_tp)
+                origin = lax.rem(me + n - k, n)
+                origin_tp = lax.rem(tp + n_tp - t, n_tp)
+                i = t * n + k
+                device = {"ep": peer, "tp": peer_tp}
+                copy = pltpu.make_async_remote_copy(
+                    src_ref=src(peer_tp, peer), dst_ref=dst(tp, me), send_sem=ssem.at[i],
+                    recv_sem=rsem.at[i], device_id=device, device_id_type=MESH,
+                )
+                copy.start()
+                sent.append(copy)
+                arrivals.append(
+                    pltpu.make_async_remote_copy(
+                        src_ref=src(peer_tp, peer), dst_ref=dst(origin_tp, origin), send_sem=ssem.at[i],
+                        recv_sem=rsem.at[i], device_id=device, device_id_type=MESH,
+                    )
+                )
+        return arrivals
+
+    def arrive(arrivals):
+        for copy in arrivals:
+            copy.wait_recv()
+
+    got = exchange(lambda j: xs.at[j], lambda j: xr.at[j], s_p1, r_p1)
+    inv_attn = lax.rsqrt(jnp.sum(x32[...] * x32[...], axis=1, keepdims=True) / d_model + EPS)
+    for copy in l_qkv:
+        copy.wait()
+    arrive(got)
+    gain_a = g_attn[:, pl.ds(pl.multiple_of(me * width, 128), width)]
+    scaled = (xr[...].reshape(allrows, width).astype(F32) * gain_a).astype(BF)
+    p2s[...] = fdot(scaled, wqkv[...]).astype(BF).reshape(p2s.shape)
+    p2r[me] = p2s[me]
+    got = exchange(lambda j: p2s.at[j], lambda j: p2r.at[j], s_p2, r_p2)
+
+    row = iota((tok * heads, 1), 0)
+    head_of_row = lax.rem(row, heads)
+    seq_of_row = row // heads
+    off_col = jnp.sum(
+        jnp.where(iota((tok * heads, heads), 1) == head_of_row, jnp.broadcast_to(offs[...], (tok * heads, heads)), 0.0),
+        axis=1, keepdims=True,
+    )
+    len_col = jnp.sum(
+        jnp.where(iota((tok * heads, tok), 1) == seq_of_row, jnp.broadcast_to(lens[...], (tok * heads, tok)).astype(F32), 0.0),
+        axis=1, keepdims=True,
+    )
+    group_col = head_of_row // per_group
+    fold = (lax.rem(iota((qcols, 2 * HEAD), 0), HEAD) == iota((qcols, 2 * HEAD), 1)).astype(F32).astype(BF)
+    unfold = (lax.rem(iota((2 * HEAD, qcols), 1), HEAD) + HEAD == iota((2 * HEAD, qcols), 0)).astype(F32).astype(BF)
+    head_mask = (iota((1, heads, qcols), 2) // HEAD == iota((1, heads, qcols), 1)).astype(F32)
+    blk = 2 * 128
+    later = (iota((blk, blk), 0) > iota((blk, blk), 1)).astype(F32).astype(BF)
+    oh[...] = jnp.zeros_like(oh)
+
+    arrive(got)
+    qkv = jnp.sum(p2r[...].astype(F32), axis=0) * inv_attn
+    q = qkv[:, :qcols].astype(BF).astype(F32)
+    key = qkv[:, qcols : qcols + kcols]
+    val = qkv[:, qcols + kcols :]
+    parts = []
+    for g in range(kv_local):
+        parts += [key[:, g * HEAD : (g + 1) * HEAD], val[:, g * HEAD : (g + 1) * HEAD]]
+    new_rows[...] = jnp.concatenate(parts, axis=1)[0:tok, :].astype(BF)
+
+    spread = (q[:, None, :] * head_mask).reshape(ROWS * heads, qcols).astype(BF)
+    q8 = fdot(spread, fold) * HEAD ** (-0.5)
+    for s in range(tok):
+        l_kv[s].wait()
+        sc[s * heads : (s + 1) * heads, :] = lax.dot_general(
+            q8[s * heads : (s + 1) * heads, :].astype(BF), kv[s],
+            (((1,), (1,)), ((), ())), preferred_element_type=F32,
+        )
+    carry = jnp.zeros((tok * heads, 1), F32)
+    for b in reversed(range(span // blk)):
+        x = sc[:, b * blk : (b + 1) * blk] - off_col
+        where_to = iota((tok * heads, blk), 1) + b * blk
+        alive = ((where_to // kv_local).astype(F32) < len_col) & (lax.rem(where_to, kv_local) == group_col)
+        tail = jnp.log(1.0 + jnp.exp(-jnp.abs(x)))
+        remain = jnp.where(alive, -(jnp.maximum(x, 0.0) + tail), 0.0)
+        high = remain.astype(BF)
+        low = (remain - high.astype(F32)).astype(BF)
+        suffix = fdot(high, later) + fdot(low, later) + carry
+        st[:, b * blk : (b + 1) * blk] = jnp.where(alive, jnp.exp(jnp.minimum(x, 0.0) - tail + suffix), 0.0)
+        carry = carry + jnp.sum(remain, axis=1, keepdims=True)
+    for s in range(tok):
+        oh[s * heads : (s + 1) * heads, :] = fdot(st[s * heads : (s + 1) * heads, :].astype(BF), kv[s])
+    wide = fdot(oh[...].astype(BF), unfold).reshape(ROWS, heads, qcols) * head_mask
+    ags[...] = jnp.sum(wide, axis=1).astype(BF)
+    agr[me] = ags[...]
+    got = exchange(lambda j: ags, lambda j: agr.at[j], s_ag, r_ag)
+    l_wo.wait()
+
+    cgrid = iota((n * SLOTS, ROWS), 0)
+    named = jnp.zeros((n * SLOTS, ROWS), F32)
+    weight = jnp.zeros((n * SLOTS, ROWS), F32)
+    for k in range(TOPK):
+        hit = rts[k : k + 1, :] == cgrid // SLOTS
+        named = named + jnp.where(hit, 1.0, 0.0)
+        weight = weight + jnp.where(hit, jnp.broadcast_to(rws[k : k + 1, :], hit.shape), 0.0)
+    before = (iota((ROWS, ROWS), 0) < iota((ROWS, ROWS), 1)).astype(F32).astype(BF)
+    slot = fdot(named.astype(BF), before)
+    pick = jnp.where(slot == lax.rem(cgrid, SLOTS).astype(F32), named, 0.0)
+    weight = weight * pick
+    pick = pick.astype(BF)
+
+    arrive(got)
+    p5s[...] = fdot(agr[...].reshape(allrows, qcols), wo[...]).astype(BF).reshape(p5s.shape)
+    p5r[tp, me] = p5s[me]
+    arrive(exchange_tp(lambda t, j: p5s.at[j], lambda t, j: p5r.at[t, j], s_p5, r_p5))
+
+    square = jnp.zeros((ROWS, 1), F32)
+    for j in range(n):
+        added = x32[:, j * width : (j + 1) * width]
+        attn = p5r[0, j].astype(F32)
+        for t in range(1, n_tp):
+            attn = attn + p5r[t, j].astype(F32)
+        mid = (added + attn).astype(BF).astype(F32)
+        rm[j] = mid
+        square = square + jnp.sum(mid * mid, axis=1, keepdims=True)
+    inv_moe = lax.rsqrt(square / d_model + EPS)
+    for j in range(n):
+        nss[j] = (rm[j] * inv_moe * g_moe[:, j * width : (j + 1) * width]).astype(BF)
+    nsr[me] = nss[me]
+    got_n = exchange(lambda j: nss.at[j], lambda j: nsr.at[j], s_n, r_n)
+    for j in range(n):
+        dsp[:, :, j * width : (j + 1) * width] = fdot(pick, nss[j]).reshape(n, SLOTS, width).astype(BF)
+    dsr[me] = dsp[me]
+    got_d = exchange(lambda j: dsp.at[j], lambda j: dsr.at[j], s_d, r_d)
+
+    for copy in l_gus:
+        copy.wait()
+    arrive(got_n)
+    s1s[...] = fdot(nsr[...].reshape(allrows, width), gus[...]).astype(BF).reshape(s1s.shape)
+    s1r[me] = s1s[me]
+    got_s1 = exchange(lambda j: s1s.at[j], lambda j: s1r.at[j], s_s1, r_s1)
+    for copy in l_exp:
+        copy.wait()
+    l_ds.wait()
+    arrive(got_s1)
+    both = jnp.sum(s1r[...].astype(F32), axis=0)
+    hs[...] = (jax.nn.silu(both[:, :fs_cols]) * both[:, fs_cols:]).astype(BF)
+    hr[me] = hs[...]
+    got_s2 = exchange(lambda j: hs, lambda j: hr.at[j], s_s2, r_s2)
+
+    arrive(got_d)
+    rows_in = dsr[...].astype(F32).reshape(n * SLOTS, d_model).astype(BF)
+    hidden = (jax.nn.silu(fdot(rows_in, ge[...])) * fdot(rows_in, ue[...])).astype(BF)
+    half = d_model // n_tp
+    for t in range(n_tp):
+        fs[t] = fdot(hidden, de[:, t * half : (t + 1) * half]).reshape(n, SLOTS, half).astype(BF)
+    fr[tp, me] = fs[tp, me]
+    got_f = exchange_tp(lambda t, j: fs.at[t, j], lambda t, j: fr.at[t, j], s_f, r_f)
+
+    arrive(got_s2)
+    f2s[...] = fdot(hr[...].reshape(allrows, fs_cols), dsh[...]).astype(BF).reshape(f2s.shape)
+    f2r[tp, me] = f2s[me]
+    got_f2 = exchange_tp(lambda t, j: f2s.at[j], lambda t, j: f2r.at[t, j], s_f2, r_f2)
+    arrive(got_f)
+    back = fr[0].astype(F32)
+    for t in range(1, n_tp):
+        back = back + fr[t].astype(F32)
+    back = back.astype(BF).astype(F32).reshape(n * SLOTS, half)
+    routed = lax.dot_general(
+        weight, back, (((0,), (0,)), ((), ())), preferred_element_type=F32, precision=lax.Precision.HIGHEST
+    )
+    arrive(got_f2)
+    chunks = n // n_tp
+    for c in range(chunks):
+        j = tp * chunks + c
+        shared = f2r[0, j].astype(F32)
+        for t in range(1, n_tp):
+            shared = shared + f2r[t, j].astype(F32)
+        total = rm[j] + shared + routed[:, c * width : (c + 1) * width]
+        out[:, c * width : (c + 1) * width] = total[0:tok, :].astype(BF)
+    for copy in sent:
+        copy.wait_send()
+
+
+def fused(
+    resid_in, norm_attn, norm_moe, w_query, w_key, w_value, head_offset, kv_cache, lengths,
+    w_output, routes, route_weights, gate_experts, up_experts, down_experts,
+    gate_shared, up_shared, down_shared,
+):
+    n = lax.axis_size("ep")
+    n_tp = lax.axis_size("tp")
+    tok, d_model = resid_in.shape
+    width = d_model // n
+    qcols, kcols = w_query.shape[1], w_key.shape[1]
+    heads = head_offset.shape[0]
+    length, kv_local = kv_cache.shape[1:3]
+    span = length * kv_local
+    fe, fs_cols = gate_experts.shape[2], gate_shared.shape[1]
+    half = d_model // n_tp
+    qkv = qcols + 2 * kcols
+    V = pltpu.VMEM
+    dma = pltpu.SemaphoreType.DMA
+    scratch = [
+        V((width, qkv), BF), V((tok, span, 2 * HEAD), BF), V(w_output.shape, BF),
+        V((d_model, fe), BF), V((d_model, fe), BF), V((fe, d_model), BF),
+        V((width, 2 * fs_cols), BF), V(down_shared.shape, BF),
+        V((ROWS, d_model), F32), V((n, ROWS, width), BF), V((n, ROWS, width), BF),
+        V((n, ROWS, qkv), BF), V((n, ROWS, qkv), BF),
+        V((tok * heads, span), F32), V((tok * heads, span), F32), V((ROWS * heads, 2 * HEAD), F32),
+        V((ROWS, qcols), BF), V((n, ROWS, qcols), BF),
+        V((n, ROWS, width), BF), V((n_tp, n, ROWS, width), BF), V((n, ROWS, width), F32),
+        V((n, SLOTS, d_model), BF), V((n, SLOTS, d_model), BF),
+        V((n, ROWS, width), BF), V((n, ROWS, width), BF),
+        V((n, ROWS, 2 * fs_cols), BF), V((n, ROWS, 2 * fs_cols), BF),
+        V((ROWS, fs_cols), BF), V((n, ROWS, fs_cols), BF),
+        V((n_tp, n, SLOTS, half), BF), V((n_tp, n, SLOTS, half), BF),
+        V((n, ROWS, width), BF), V((n_tp, n, ROWS, width), BF),
+        V((TOPK, ROWS), jnp.int32), V((TOPK, ROWS), F32),
+        dma((10 + tok,)),
+    ]
+    scratch += [dma((n,))] * 6 + [dma((n_tp * n,))] * 2 + [dma((n,))] * 8 + [dma((n_tp * n,))] * 4
+    in_vmem = pl.BlockSpec(memory_space=pltpu.VMEM)
+    in_hbm = pl.BlockSpec(memory_space=pl.ANY)
+    out, rows = pl.pallas_call(
+        functools.partial(layer_kernel, n, n_tp, tok),
+        out_shape=(
+            jax.ShapeDtypeStruct((tok, half), BF),
+            jax.ShapeDtypeStruct((tok, 2 * kcols), BF),
+        ),
+        in_specs=[in_vmem] * 7 + [in_hbm] * 11,
+        out_specs=(in_vmem, in_vmem),
+        scratch_shapes=scratch,
+        compiler_params=pltpu.CompilerParams(
+            collective_id=0, has_side_effects=True, vmem_limit_bytes=60 * 2**20
+        ),
+    )(
+        resid_in, norm_attn.reshape(1, -1), norm_moe.reshape(1, -1), head_offset.reshape(1, -1),
+        lengths.reshape(1, -1), routes.T, route_weights.T,
+        w_query, w_key, w_value, kv_cache.reshape(tok, span, 2 * HEAD), w_output,
+        gate_experts, up_experts, down_experts, gate_shared, up_shared, down_shared,
+    )
+    return out, rows.reshape(tok, kv_local, 2 * HEAD)
+
+
+def layer(*args):
+    n = lax.axis_size("ep")
+    n_tp = lax.axis_size("tp")
+    tok, d_model = args[0].shape
+    local_experts = args[12].shape[0]
+    capacity = min(tok, tok * TOPK // (local_experts * n) + 2)
+    fits = (
+        tok <= ROWS
+        and local_experts == 1
+        and capacity <= SLOTS
+        and d_model % (128 * n) == 0
+        and n % n_tp == 0
+    )
+    return fused(*args) if fits else on_device(*args)
+
+
 def solution(mesh):
     return jax.shard_map(
-        on_device,
+        layer,
         mesh=mesh,
         in_specs=(
             P(("grp", "ep"), None),

time: 271 us -> 61.1 us (0.23)
  other arithmetic: 113 us -> 0 us
  Pallas kernels: 0 us -> 57.5 us
  blocking collectives: 53.2 us -> 0 us
  waiting for transfers between devices: 48.6 us -> 0 us
  matrix products: 20.8 us -> 0 us
  local copies, waits for them, and re-layouts: 16.5 us -> 2.68 us
  between operations: 14.4 us -> 0.65 us
  starting transfers between devices: 3.64 us -> 0 us
    another operation x4 -> x0, other arithmetic: 109 us -> none
    pallas_call x0 -> x1, Pallas kernels: none -> 57.5 us  [fused(): pl.pallas_call(functools.partial(layer_kernel, n, n_tp, tok), out_shape=(...]
    all_gather x5 -> x0, waiting for transfers between devices: 37 us -> none  [the longest x1 19.6 us: on_device(): lax.all_gather(down_shared, 'ep', axis=1, tiled=True)]
    all_gather x2 -> x0, blocking collectives: 31.8 us -> none  [the longest x1 16.9 us: on_device(): lax.all_gather(w_value, 'ep', axis=0, tiled=True)]
    dot_general x13 -> x0, matrix products: 20.8 us -> none  [the longest x1 4.4 us: stick_read(): jnp.einsum('skgl,slkd->skgd', stick, value_rows, preferred_element_type=j...]
    slice x2 -> x0, local copies, waits for them, and re-layouts: 13.4 us -> none  [the longest x1 12.9 us: stick_read(): key_rows = kv_cache[:, :, :, :HEAD]]
    all_to_all x1 -> x0, blocking collectives: 12.6 us -> none  [on_device(): lax.all_to_all(outgoing, 'ep', split_axis=0, concat_axis=0, tiled=True)]
    psum x1 -> x0, blocking collectives: 8.79 us -> none  [on_device(): attn_sum = lax.psum(attn_part, 'tp').astype(jnp.float32)]
  transfers between devices with their start and end apart: 8 -> 0, of which waited for: 3 -> 0; matrix products, arithmetic and copies ran while one was open for 55% -> 0% of each run, Pallas kernels for 0% -> 0%
where the time goes in v1:
time: 61.1 us; the launch traced here: 60.8 us
  Pallas kernels  57.5 us (94%)
  local copies, waits for them, and re-layouts  2.68 us (4%)
  between operations  0.65 us (1%)
    pallas_call x1, Pallas kernels, fused(): pl.pallas_call(functools.partial(layer_kernel, n, n_tp, tok), out_shape=(...  57.5 us
    unnamed x1, local copies, waits for them, and re-layouts  1.37 us
    reshape x1, local copies, waits for them, and re-layouts, fused(): return (out, rows.reshape(tok, kv_local, 2 * HEAD))  1.31 us

profile of v1, /device:TPU:0, one launch (start us, length us, event | category | flops | bytes accessed | tf_op | source)
XLA Modules:
  0.0 60.8 jit_solution(2846637548950078795)
XLA Ops:
  0.6 57.5 %shard_map.185 = (bf16[11,1024]{1,0:T(8,128)(2,1)}, bf16[11,256]{1,0:T(8,128)(2,1)}) custom-call(bf16[11,2048]{1,0:T(8,128)(2,1)} %resid.1, f32[1,2048]{1,0:T(1,128)} %bitcast.8, f32[1,2048]{1,0:T(1,128)} %bitcast.9, f32[1,8]{1,0:T(1,128)} %bitcast.12, s32[1,11]{1,0:T(1,128)} %bitcast.13, s32[4,11]{1,0:T(4,128)} %bitcast.10, f32[4,11]{1,0:T(4,128)} %bitcast.11, ...), custom_call_target="tpu_custom_call" | custom-call | tf_op jit(solution)/shard_map/pallas_call | solution.py:478
  58.1 1.3 %reshape.27 = bf16[11,2,128]{2,1,0:T(2,128)(2,1)} reshape(bf16[11,256]{1,0:T(8,128)(2,1)} %get-tuple-element.5) | data formatting | bytes 11264 | tf_op jit(solution)/shard_map/reshape | solution.py:496
  59.4 1.4 %copy.21 = bf16[11,1024]{1,0:T(8,128)(2,1)} copy(bf16[11,1024]{1,0:T(8,128)(2,1)} %get-tuple-element.8) | data formatting | bytes 45056

commit v2 on v1

--- a/solution.py
+++ b/solution.py
@@ -171,9 +171,9 @@
     wq_h, wk_h, wv_h, kv_h, wo_h, ge_h, ue_h, de_h, gs_h, us_h, ds_h,
     out, new_rows,
     wqkv, kv, wo, ge, ue, de, gus, dsh,
-    x32, xs, xr, p2s, p2r, sc, st, oh, ags, agr, p5s, p5r, rm, dsp, dsr, nss, nsr,
+    x32, xs, xr, p2s, p2r, sc, st, oh, ags, agr, xps, xpr, dsp, dsr,
     s1s, s1r, hs, hr, fs, fr, f2s, f2r, rts, rws,
-    lsem, s_p1, r_p1, s_p2, r_p2, s_ag, r_ag, s_p5, r_p5, s_d, r_d, s_n, r_n,
+    lsem, s_p1, r_p1, s_p2, r_p2, s_ag, r_ag, s_x, r_x, s_d, r_d,
     s_s1, r_s1, s_s2, r_s2, s_f, r_f, s_f2, r_f2,
 ):
     me = lax.axis_index("ep")
@@ -221,13 +221,18 @@
 
     x32[...] = jnp.zeros_like(x32)
     x32[0:tok, :] = resid[...].astype(F32)
-    for j in range(n):
-        xs[j] = x32[:, j * width : (j + 1) * width].astype(BF)
-    xr[me] = xs[me]
-    rts[...] = jnp.full(rts.shape, -1, jnp.int32)
-    rts[:, 0:tok] = routes[...]
+    rts[...] = jnp.full(rts.shape, -1.0, F32)
+    rts[:, 0:tok] = routes[...].astype(F32)
     rws[...] = jnp.zeros_like(rws)
     rws[:, 0:tok] = rweights[...]
+    spot = (iota((TOPK, 128), 0) == iota((TOPK, 128), 1)).astype(F32)
+    routes_rows = lax.dot_general(
+        rts[...], spot, (((0,), (0,)), ((), ())), preferred_element_type=F32
+    ).astype(BF)
+    for j in range(n):
+        xs[j, :, 0:width] = x32[:, j * width : (j + 1) * width].astype(BF)
+        xs[j, :, width:] = routes_rows
+    xr[me] = xs[me]
 
     pl.semaphore_wait(barrier, n * n_tp - 1)
 
@@ -288,7 +293,7 @@
         copy.wait()
     arrive(got)
     gain_a = g_attn[:, pl.ds(pl.multiple_of(me * width, 128), width)]
-    scaled = (xr[...].reshape(allrows, width).astype(F32) * gain_a).astype(BF)
+    scaled = (xr[:, :, 0:width].reshape(allrows, width).astype(F32) * gain_a).astype(BF)
     p2s[...] = fdot(scaled, wqkv[...]).astype(BF).reshape(p2s.shape)
     p2r[me] = p2s[me]
     got = exchange(lambda j: p2s.at[j], lambda j: p2r.at[j], s_p2, r_p2)
@@ -354,56 +359,83 @@
     named = jnp.zeros((n * SLOTS, ROWS), F32)
     weight = jnp.zeros((n * SLOTS, ROWS), F32)
     for k in range(TOPK):
-        hit = rts[k : k + 1, :] == cgrid // SLOTS
+        hit = rts[k : k + 1, :] == (cgrid // SLOTS).astype(F32)
         named = named + jnp.where(hit, 1.0, 0.0)
         weight = weight + jnp.where(hit, jnp.broadcast_to(rws[k : k + 1, :], hit.shape), 0.0)
     before = (iota((ROWS, ROWS), 0) < iota((ROWS, ROWS), 1)).astype(F32).astype(BF)
     slot = fdot(named.astype(BF), before)
     pick = jnp.where(slot == lax.rem(cgrid, SLOTS).astype(F32), named, 0.0)
     weight = weight * pick
-    pick = pick.astype(BF)
+    per_expert = n * SLOTS
+    all_routes = xr[:, :, width:].reshape(allrows, 128).astype(F32).T
+    rgrid = iota((n * per_expert, allrows), 0)
+    qgrid = iota((n * per_expert, allrows), 1)
+    want = (rgrid // per_expert).astype(F32)
+    named_all = jnp.zeros((n * per_expert, allrows), F32)
+    for k in range(TOPK):
+        named_all = named_all + jnp.where(all_routes[k : k + 1, :] == want, 1.0, 0.0)
+    qa, qb = iota((allrows, allrows), 0), iota((allrows, allrows), 1)
+    before_all = jnp.where((qa // ROWS == qb // ROWS) & (qa < qb), 1.0, 0.0).astype(BF)
+    slot_all = fdot(named_all.astype(BF), before_all)
+    right = (lax.rem(rgrid, per_expert) // SLOTS == qgrid // ROWS) & (
+        slot_all == lax.rem(rgrid, SLOTS).astype(F32)
+    )
+    pick_all = jnp.where(right, named_all, 0.0).astype(BF)
 
     arrive(got)
-    p5s[...] = fdot(agr[...].reshape(allrows, qcols), wo[...]).astype(BF).reshape(p5s.shape)
-    p5r[tp, me] = p5s[me]
-    arrive(exchange_tp(lambda t, j: p5s.at[j], lambda t, j: p5r.at[t, j], s_p5, r_p5))
-
-    square = jnp.zeros((ROWS, 1), F32)
-    for j in range(n):
-        added = x32[:, j * width : (j + 1) * width]
-        attn = p5r[0, j].astype(F32)
-        for t in range(1, n_tp):
-            attn = attn + p5r[t, j].astype(F32)
-        mid = (added + attn).astype(BF).astype(F32)
-        rm[j] = mid
-        square = square + jnp.sum(mid * mid, axis=1, keepdims=True)
-    inv_moe = lax.rsqrt(square / d_model + EPS)
-    for j in range(n):
-        nss[j] = (rm[j] * inv_moe * g_moe[:, j * width : (j + 1) * width]).astype(BF)
-    nsr[me] = nss[me]
-    got_n = exchange(lambda j: nss.at[j], lambda j: nsr.at[j], s_n, r_n)
-    for j in range(n):
-        dsp[:, :, j * width : (j + 1) * width] = fdot(pick, nss[j]).reshape(n, SLOTS, width).astype(BF)
+    part = fdot(agr[...].reshape(allrows, qcols), wo[...]).astype(BF)
+    xps[...] = part
+    swap = pltpu.make_async_remote_copy(
+        src_ref=xps, dst_ref=xpr, send_sem=s_x.at[0], recv_sem=r_x.at[0],
+        device_id={"tp": lax.rem(tp + 1, n_tp)}, device_id_type=MESH,
+    )
+    swap.start()
+    sent.append(swap)
+    gain_m = g_moe[:, pl.ds(pl.multiple_of(me * width, 128), width)]
+    base = xr[:, :, 0:width].reshape(allrows, width).astype(F32)
+    for copy in l_gus:
+        copy.wait()
+    swap.wait_recv()
+    mid = (base + (part.astype(F32) + xpr[...].astype(F32))).astype(BF)
+    mid32 = mid.astype(F32)
+
+    square = jnp.sum(mid32 * mid32, axis=1, keepdims=True)
+    sq_high = square.astype(BF).astype(F32)
+    lane = iota((allrows, 128), 1)
+    sq_wide = jnp.where(lane == 0, sq_high, jnp.where(lane == 1, square - sq_high, 0.0))
+    s1s[:, :, 0 : 2 * fs_cols] = fdot((mid32 * gain_m).astype(BF), gus[...]).astype(BF).reshape(n, ROWS, 2 * fs_cols)
+    s1s[:, :, 2 * fs_cols :] = sq_wide.astype(BF).reshape(n, ROWS, 128)
+    s1r[me] = s1s[me]
+    got_s1 = exchange(lambda j: s1s.at[j], lambda j: s1r.at[j], s_s1, r_s1)
+    dsp[...] = fdot(pick_all, mid).astype(BF).reshape(dsp.shape)
     dsr[me] = dsp[me]
     got_d = exchange(lambda j: dsp.at[j], lambda j: dsr.at[j], s_d, r_d)
 
-    for copy in l_gus:
-        copy.wait()
-    arrive(got_n)
-    s1s[...] = fdot(nsr[...].reshape(allrows, width), gus[...]).astype(BF).reshape(s1s.shape)
-    s1r[me] = s1s[me]
-    got_s1 = exchange(lambda j: s1s.at[j], lambda j: s1r.at[j], s_s1, r_s1)
     for copy in l_exp:
         copy.wait()
     l_ds.wait()
     arrive(got_s1)
-    both = jnp.sum(s1r[...].astype(F32), axis=0)
+    inv_own = lax.rsqrt(
+        jnp.sum(jnp.sum(s1r[:, :, 2 * fs_cols :].astype(F32), axis=0), axis=1, keepdims=True) / d_model + EPS
+    )
+    both = jnp.sum(s1r[:, :, 0 : 2 * fs_cols].astype(F32), axis=0) * inv_own
     hs[...] = (jax.nn.silu(both[:, :fs_cols]) * both[:, fs_cols:]).astype(BF)
     hr[me] = hs[...]
     got_s2 = exchange(lambda j: hs, lambda j: hr.at[j], s_s2, r_s2)
 
     arrive(got_d)
-    rows_in = dsr[...].astype(F32).reshape(n * SLOTS, d_model).astype(BF)
+    square = jnp.zeros((per_expert, 1), F32)
+    for j in range(n):
+        piece = dsr[j].astype(F32)
+        square = square + jnp.sum(piece * piece, axis=1, keepdims=True)
+    inv_moe = lax.rsqrt(square / d_model + EPS)
+    rows_in = jnp.concatenate(
+        [
+            (dsr[j].astype(F32) * inv_moe * g_moe[:, j * width : (j + 1) * width]).astype(BF)
+            for j in range(n)
+        ],
+        axis=1,
+    )
     hidden = (jax.nn.silu(fdot(rows_in, ge[...])) * fdot(rows_in, ue[...])).astype(BF)
     half = d_model // n_tp
     for t in range(n_tp):
@@ -412,9 +444,30 @@
     got_f = exchange_tp(lambda t, j: fs.at[t, j], lambda t, j: fr.at[t, j], s_f, r_f)
 
     arrive(got_s2)
-    f2s[...] = fdot(hr[...].reshape(allrows, fs_cols), dsh[...]).astype(BF).reshape(f2s.shape)
-    f2r[tp, me] = f2s[me]
-    got_f2 = exchange_tp(lambda t, j: f2s.at[j], lambda t, j: f2r.at[t, j], s_f2, r_f2)
+    chunks = n // n_tp
+    target = me // chunks
+    chunk = lax.rem(me, chunks)
+    carried = jnp.where(tp == 0, 1.0, 0.0) * mid32
+    f2s[...] = (fdot(hr[...].reshape(allrows, fs_cols), dsh[...]) + carried).astype(BF).reshape(f2s.shape)
+
+    def give(k):
+        peer = lax.rem(me + k, n)
+        return pltpu.make_async_remote_copy(
+            src_ref=f2s.at[peer], dst_ref=f2r.at[tp, chunk], send_sem=s_f2.at[k],
+            recv_sem=r_f2.at[chunk * n_tp + tp], device_id={"ep": peer, "tp": target}, device_id_type=MESH,
+        )
+
+    for k in range(1, n):
+        give(k).start()
+
+    @pl.when(target != tp)
+    def _():
+        give(0).start()
+
+    @pl.when(target == tp)
+    def _():
+        f2r[tp, chunk] = f2s[me]
+
     arrive(got_f)
     back = fr[0].astype(F32)
     for t in range(1, n_tp):
@@ -423,15 +476,28 @@
     routed = lax.dot_general(
         weight, back, (((0,), (0,)), ((), ())), preferred_element_type=F32, precision=lax.Precision.HIGHEST
     )
-    arrive(got_f2)
-    chunks = n // n_tp
     for c in range(chunks):
-        j = tp * chunks + c
-        shared = f2r[0, j].astype(F32)
-        for t in range(1, n_tp):
-            shared = shared + f2r[t, j].astype(F32)
-        total = rm[j] + shared + routed[:, c * width : (c + 1) * width]
+        for t in range(n_tp):
+
+            @pl.when((tp * chunks + c != me) | (tp != t))
+            def _():
+                pltpu.make_async_remote_copy(
+                    src_ref=f2s.at[me], dst_ref=f2r.at[t, c], send_sem=s_f2.at[0],
+                    recv_sem=r_f2.at[c * n_tp + t], device_id={"tp": 1 - tp}, device_id_type=MESH,
+                ).wait_recv()
+
+    for c in range(chunks):
+        total = routed[:, c * width : (c + 1) * width]
+        for t in range(n_tp):
+            total = total + f2r[t, c].astype(F32)
         out[:, c * width : (c + 1) * width] = total[0:tok, :].astype(BF)
+    for k in range(1, n):
+        give(k).wait_send()
+
+    @pl.when(target != tp)
+    def _():
+        give(0).wait_send()
+
     for copy in sent:
         copy.wait_send()
 
@@ -458,21 +524,20 @@
         V((width, qkv), BF), V((tok, span, 2 * HEAD), BF), V(w_output.shape, BF),
         V((d_model, fe), BF), V((d_model, fe), BF), V((fe, d_model), BF),
         V((width, 2 * fs_cols), BF), V(down_shared.shape, BF),
-        V((ROWS, d_model), F32), V((n, ROWS, width), BF), V((n, ROWS, width), BF),
+        V((ROWS, d_model), F32), V((n, ROWS, width + 128), BF), V((n, ROWS, width + 128), BF),
         V((n, ROWS, qkv), BF), V((n, ROWS, qkv), BF),
         V((tok * heads, span), F32), V((tok * heads, span), F32), V((ROWS * heads, 2 * HEAD), F32),
         V((ROWS, qcols), BF), V((n, ROWS, qcols), BF),
-        V((n, ROWS, width), BF), V((n_tp, n, ROWS, width), BF), V((n, ROWS, width), F32),
-        V((n, SLOTS, d_model), BF), V((n, SLOTS, d_model), BF),
-        V((n, ROWS, width), BF), V((n, ROWS, width), BF),
-        V((n, ROWS, 2 * fs_cols), BF), V((n, ROWS, 2 * fs_cols), BF),
+        V((n * ROWS, width), BF), V((n * ROWS, width), BF),
+        V((n, n * SLOTS, width), BF), V((n, n * SLOTS, width), BF),
+        V((n, ROWS, 2 * fs_cols + 128), BF), V((n, ROWS, 2 * fs_cols + 128), BF),
         V((ROWS, fs_cols), BF), V((n, ROWS, fs_cols), BF),
         V((n_tp, n, SLOTS, half), BF), V((n_tp, n, SLOTS, half), BF),
-        V((n, ROWS, width), BF), V((n_tp, n, ROWS, width), BF),
-        V((TOPK, ROWS), jnp.int32), V((TOPK, ROWS), F32),
+        V((n, ROWS, width), BF), V((n_tp, n // n_tp, ROWS, width), BF),
+        V((TOPK, ROWS), F32), V((TOPK, ROWS), F32),
         dma((10 + tok,)),
     ]
-    scratch += [dma((n,))] * 6 + [dma((n_tp * n,))] * 2 + [dma((n,))] * 8 + [dma((n_tp * n,))] * 4
+    scratch += [dma((n,))] * 6 + [dma((1,))] * 2 + [dma((n,))] * 6 + [dma((n_tp * n,))] * 2 + [dma((n,))] * 2
     in_vmem = pl.BlockSpec(memory_space=pltpu.VMEM)
     in_hbm = pl.BlockSpec(memory_space=pl.ANY)
     out, rows = pl.pallas_call(
@@ -501,13 +566,16 @@
     n_tp = lax.axis_size("tp")
     tok, d_model = args[0].shape
     local_experts = args[12].shape[0]
-    capacity = min(tok, tok * TOPK // (local_experts * n) + 2)
+    experts_all = local_experts * n
+    capacity = min(tok, tok * TOPK // experts_all + 2)
     fits = (
         tok <= ROWS
         and local_experts == 1
         and capacity <= SLOTS
         and d_model % (128 * n) == 0
         and n % n_tp == 0
+        and n_tp == 2
+        and experts_all <= 128
     )
     return fused(*args) if fits else on_device(*args)
 

time: 61.1 us -> 54.1 us (0.89)
  Pallas kernels: 57.5 us -> 50.3 us
    pallas_call x1, Pallas kernels: 57.5 us -> 50.3 us  [fused(): pl.pallas_call(functools.partial(layer_kernel, n, n_tp, tok), out_shape=(...]
where the time goes in v2:
time: 54.1 us; the launch traced here: 53.7 us
  Pallas kernels  50.3 us (93%)
  local copies, waits for them, and re-layouts  2.68 us (5%)
  between operations  0.65 us (1%)
    pallas_call x1, Pallas kernels, fused(): pl.pallas_call(functools.partial(layer_kernel, n, n_tp, tok), out_shape=(...  50.3 us
    unnamed x1, local copies, waits for them, and re-layouts  1.37 us
    reshape x1, local copies, waits for them, and re-layouts, fused(): return (out, rows.reshape(tok, kv_local, 2 * HEAD))  1.31 us

profile of v2, /device:TPU:0, one launch (start us, length us, event | category | flops | bytes accessed | tf_op | source)
XLA Modules:
  0.0 53.7 jit_solution(4375771479104926527)
XLA Ops:
  0.6 50.3 %shard_map.185 = (bf16[11,1024]{1,0:T(8,128)(2,1)}, bf16[11,256]{1,0:T(8,128)(2,1)}) custom-call(bf16[11,2048]{1,0:T(8,128)(2,1)} %resid.1, f32[1,2048]{1,0:T(1,128)} %bitcast.8, f32[1,2048]{1,0:T(1,128)} %bitcast.9, f32[1,8]{1,0:T(1,128)} %bitcast.12, s32[1,11]{1,0:T(1,128)} %bitcast.13, s32[4,11]{1,0:T(4,128)} %bitcast.10, f32[4,11]{1,0:T(4,128)} %bitcast.11, ...), custom_call_target="tpu_custom_call" | custom-call | tf_op jit(solution)/shard_map/pallas_call | solution.py:543
  51.0 1.3 %reshape.27 = bf16[11,2,128]{2,1,0:T(2,128)(2,1)} reshape(bf16[11,256]{1,0:T(8,128)(2,1)} %get-tuple-element.5) | data formatting | bytes 11264 | tf_op jit(solution)/shard_map/reshape | solution.py:561
  52.3 1.4 %copy.21 = bf16[11,1024]{1,0:T(8,128)(2,1)} copy(bf16[11,1024]{1,0:T(8,128)(2,1)} %get-tuple-element.8) | data formatting | bytes 45056

commit v3 on v2

--- a/solution.py
+++ b/solution.py
@@ -167,10 +167,10 @@
 
 
 def layer_kernel(
-    n, n_tp, tok, resid, g_attn, g_moe, offs, lens, routes, rweights,
+    n, n_tp, tok, resid_h, g_attn_h, g_moe_h, offs_h, lens_h, routes_h, rweights_h,
     wq_h, wk_h, wv_h, kv_h, wo_h, ge_h, ue_h, de_h, gs_h, us_h, ds_h,
-    out, new_rows,
-    wqkv, kv, wo, ge, ue, de, gus, dsh,
+    out_h, new_rows_h,
+    resid, g_attn, g_moe, offs, lens, routes, rweights, out, new_rows, osem, wqkv, kv, wo, ge, ue, de, gus, dsh,
     x32, xs, xr, p2s, p2r, sc, st, oh, ags, agr, xps, xpr, dsp, dsr,
     s1s, s1r, hs, hr, fs, fr, f2s, f2r, rts, rws,
     lsem, s_p1, r_p1, s_p2, r_p2, s_ag, r_ag, s_x, r_x, s_d, r_d,
@@ -196,6 +196,10 @@
         loads.append(copy)
         return copy
 
+    small = [
+        load(resid_h, resid), load(routes_h, routes), load(rweights_h, rweights), load(g_attn_h, g_attn),
+        load(g_moe_h, g_moe), load(offs_h, offs), load(lens_h, lens),
+    ]
     l_qkv = [
         load(wq_h, wqkv.at[:, pl.ds(0, qcols)]),
         load(wk_h, wqkv.at[:, pl.ds(qcols, kcols)]),
@@ -219,6 +223,8 @@
                     device_id_type=MESH,
                 )
 
+    for copy in small:
+        copy.wait()
     x32[...] = jnp.zeros_like(x32)
     x32[0:tok, :] = resid[...].astype(F32)
     rts[...] = jnp.full(rts.shape, -1.0, F32)
@@ -257,12 +263,10 @@
             )
         return arrivals
 
-    def exchange_tp(src, dst, ssem, rsem):
+    def exchange_tp(t, src, dst, ssem, rsem):
         arrivals = []
         for k in range(n):
-            for t in range(n_tp):
-                if not (k or t):
-                    continue
+            if k or t:
                 peer = lax.rem(me + k, n)
                 peer_tp = lax.rem(tp + t, n_tp)
                 origin = lax.rem(me + n - k, n)
@@ -326,6 +330,8 @@
     for g in range(kv_local):
         parts += [key[:, g * HEAD : (g + 1) * HEAD], val[:, g * HEAD : (g + 1) * HEAD]]
     new_rows[...] = jnp.concatenate(parts, axis=1)[0:tok, :].astype(BF)
+    put_rows = pltpu.make_async_copy(new_rows, new_rows_h, osem.at[0])
+    put_rows.start()
 
     spread = (q[:, None, :] * head_mask).reshape(ROWS * heads, qcols).astype(BF)
     q8 = fdot(spread, fold) * HEAD ** (-0.5)
@@ -438,10 +444,14 @@
     )
     hidden = (jax.nn.silu(fdot(rows_in, ge[...])) * fdot(rows_in, ue[...])).astype(BF)
     half = d_model // n_tp
-    for t in range(n_tp):
-        fs[t] = fdot(hidden, de[:, t * half : (t + 1) * half]).reshape(n, SLOTS, half).astype(BF)
-    fr[tp, me] = fs[tp, me]
-    got_f = exchange_tp(lambda t, j: fs.at[t, j], lambda t, j: fr.at[t, j], s_f, r_f)
+    got_f = []
+    for t in reversed(range(n_tp)):
+        to = lax.rem(tp + t, n_tp)
+        cols = pl.ds(pl.multiple_of(to * half, 128), half)
+        fs[to] = fdot(hidden, de[:, cols]).reshape(n, SLOTS, half).astype(BF)
+        if t == 0:
+            fr[tp, me] = fs[tp, me]
+        got_f += exchange_tp(t, lambda t, j: fs.at[t, j], lambda t, j: fr.at[t, j], s_f, r_f)
 
     arrive(got_s2)
     chunks = n // n_tp
@@ -491,6 +501,8 @@
         for t in range(n_tp):
             total = total + f2r[t, c].astype(F32)
         out[:, c * width : (c + 1) * width] = total[0:tok, :].astype(BF)
+    put_out = pltpu.make_async_copy(out, out_h, osem.at[1])
+    put_out.start()
     for k in range(1, n):
         give(k).wait_send()
 
@@ -500,6 +512,8 @@
 
     for copy in sent:
         copy.wait_send()
+    put_rows.wait()
+    put_out.wait()
 
 
 def fused(
@@ -521,6 +535,9 @@
     V = pltpu.VMEM
     dma = pltpu.SemaphoreType.DMA
     scratch = [
+        V((tok, d_model), BF), V((1, d_model), F32), V((1, d_model), F32), V((1, heads), F32),
+        V((1, tok), jnp.int32), V((TOPK, tok), jnp.int32), V((TOPK, tok), F32),
+        V((tok, half), BF), V((tok, 2 * kcols), BF), dma((2,)),
         V((width, qkv), BF), V((tok, span, 2 * HEAD), BF), V(w_output.shape, BF),
         V((d_model, fe), BF), V((d_model, fe), BF), V((fe, d_model), BF),
         V((width, 2 * fs_cols), BF), V(down_shared.shape, BF),
@@ -535,10 +552,9 @@
         V((n_tp, n, SLOTS, half), BF), V((n_tp, n, SLOTS, half), BF),
         V((n, ROWS, width), BF), V((n_tp, n // n_tp, ROWS, width), BF),
         V((TOPK, ROWS), F32), V((TOPK, ROWS), F32),
-        dma((10 + tok,)),
+        dma((17 + tok,)),
     ]
     scratch += [dma((n,))] * 6 + [dma((1,))] * 2 + [dma((n,))] * 6 + [dma((n_tp * n,))] * 2 + [dma((n,))] * 2
-    in_vmem = pl.BlockSpec(memory_space=pltpu.VMEM)
     in_hbm = pl.BlockSpec(memory_space=pl.ANY)
     out, rows = pl.pallas_call(
         functools.partial(layer_kernel, n, n_tp, tok),
@@ -546,8 +562,8 @@
             jax.ShapeDtypeStruct((tok, half), BF),
             jax.ShapeDtypeStruct((tok, 2 * kcols), BF),
         ),
-        in_specs=[in_vmem] * 7 + [in_hbm] * 11,
-        out_specs=(in_vmem, in_vmem),
+        in_specs=[in_hbm] * 18,
+        out_specs=(in_hbm, in_hbm),
         scratch_shapes=scratch,
         compiler_params=pltpu.CompilerParams(
             collective_id=0, has_side_effects=True, vmem_limit_bytes=60 * 2**20

time: 54.1 us -> 53 us (0.980)
  Pallas kernels: 50.3 us -> 49 us
    pallas_call x1, Pallas kernels: 50.3 us -> 49 us  [fused(): pl.pallas_call(functools.partial(layer_kernel, n, n_tp, tok), out_shape=(...]
where the time goes in v3:
time: 53 us; the launch traced here: 52.3 us
  Pallas kernels  49 us (92%)
  local copies, waits for them, and re-layouts  2.68 us (5%)
  between operations  0.65 us (1%)
    pallas_call x1, Pallas kernels, fused(): pl.pallas_call(functools.partial(layer_kernel, n, n_tp, tok), out_shape=(...  49 us
    unnamed x1, local copies, waits for them, and re-layouts  1.37 us
    reshape x1, local copies, waits for them, and re-layouts, fused(): return (out, rows.reshape(tok, kv_local, 2 * HEAD))  1.31 us

profile of v3, /device:TPU:0, one launch (start us, length us, event | category | flops | bytes accessed | tf_op | source)
XLA Modules:
  0.0 52.3 jit_solution(8269612758094504689)
XLA Ops:
  0.6 49.0 %shard_map.185 = (bf16[11,1024]{1,0:T(8,128)(2,1)}, bf16[11,256]{1,0:T(8,128)(2,1)}) custom-call(bf16[11,2048]{1,0:T(8,128)(2,1)} %resid_h.1, f32[1,2048]{1,0:T(1,128)} %bitcast.8, f32[1,2048]{1,0:T(1,128)} %bitcast.9, f32[1,8]{1,0:T(1,128)} %bitcast.12, s32[1,11]{1,0:T(1,128)} %bitcast.13, s32[4,11]{1,0:T(4,128)} %bitcast.10, f32[4,11]{1,0:T(4,128)} %bitcast.11, ...), custom_call_target="tpu_custom_call" | custom-call | tf_op jit(solution)/shard_map/pallas_call | solution.py:559
  49.6 1.3 %reshape.27 = bf16[11,2,128]{2,1,0:T(2,128)(2,1)} reshape(bf16[11,256]{1,0:T(8,128)(2,1)} %get-tuple-element.5) | data formatting | bytes 11264 | tf_op jit(solution)/shard_map/reshape | solution.py:577
  50.9 1.4 %copy.21 = bf16[11,1024]{1,0:T(8,128)(2,1)} copy(bf16[11,1024]{1,0:T(8,128)(2,1)} %get-tuple-element.8) | data formatting | bytes 45056
